TPU v7x, 32 devices: a whole 2x2x4 slice. The times are simulated.
32 devices in a mesh: fs: 4 (over y, x), tp: 8 (over z, core).
Axes of the slice: x: 2, y: 2, z: 4, core: 2. Of those that a mesh axis runs over, the one named last changes fastest.
Arguments:
- tokens: bfloat16 [4096, 2048], P(('fs', 'tp')), may hold values from -6 to 6
- gate_weight: bfloat16 [2048, 5632], P('fs', 'tp'), may hold values from -0.125 to 0.125
- up_weight: bfloat16 [2048, 5632], P('fs', 'tp'), may hold values from -0.125 to 0.125
- down_weight: bfloat16 [5632, 2048], P('tp', 'fs'), may hold values from -0.078125 to 0.078125
- grad_out: bfloat16 [4096, 2048], P(('fs', 'tp')), may hold values from -6 to 6
Outputs:
- grad_input: bfloat16 [4096, 2048], P(('fs', 'tp'))
- grad_gate: float32 [2048, 5632], P('fs', 'tp')
- grad_up: float32 [2048, 5632], P('fs', 'tp')
- grad_down: float32 [5632, 2048], P('tp', 'fs')
All inputs are finite; a program needn't handle non-finite values.
Results may differ from a plain program's by a relative error of at most 0.0049.
Values may be sent and summed in bfloat16 or wider, within the bound.
A program may use at most 128 MiB of HBM per device.

v0:
```python
import jax
import jax.numpy as jnp
from jax import lax
from jax.sharding import PartitionSpec as P


def over_rows(left, right):
    return lax.dot_general(
        left, right, (((0,), (0,)), ((), ())), preferred_element_type=jnp.float32
    )


def over_cols(left, right):
    return lax.dot_general(
        left, right, (((1,), (1,)), ((), ())), preferred_element_type=jnp.float32
    )


def body(tokens, gate_weight, up_weight, down_weight, grad_out):
    tok_all, cot_all = (
        lax.all_gather(tokens, "tp", axis=0, tiled=True),
        lax.all_gather(grad_out, "tp", axis=0, tiled=True),
    )
    gate_full, up_full = (
        lax.all_gather(gate_weight, "fs", axis=0, tiled=True),
        lax.all_gather(up_weight, "fs", axis=0, tiled=True),
    )
    down_full = lax.all_gather(down_weight, "fs", axis=1, tiled=True)
    gate_pre = jnp.dot(tok_all, gate_full, preferred_element_type=jnp.float32)
    up_pre = jnp.dot(tok_all, up_full, preferred_element_type=jnp.float32)
    sig_gate = jax.nn.sigmoid(gate_pre)
    active = gate_pre * sig_gate
    hidden = (active * up_pre).astype(jnp.bfloat16)
    d_hidden = over_cols(cot_all, down_full)
    d_gate = (d_hidden * up_pre * sig_gate * (1.0 + gate_pre * (1.0 - sig_gate))).astype(
        jnp.bfloat16
    )
    d_up = (d_hidden * active).astype(jnp.bfloat16)
    grad_input = lax.psum_scatter(
        over_cols(d_gate, gate_full) + over_cols(d_up, up_full),
        "tp",
        scatter_dimension=0,
        tiled=True,
    ).astype(jnp.bfloat16)
    width = gate_full.shape[1]
    summed = lax.psum_scatter(
        jnp.concatenate(
            [over_rows(tok_all, d_gate), over_rows(tok_all, d_up), over_rows(cot_all, hidden)],
            axis=1,
        ),
        "fs",
        scatter_dimension=0,
        tiled=True,
    )
    grad_gate = summed[:, :width]
    grad_up = summed[:, width : 2 * width]
    grad_down = summed[:, 2 * width :].T
    return (grad_input, grad_gate, grad_up, grad_down)


def solution(mesh):
    in_specs = (
        P(("fs", "tp"), None),
        P("fs", "tp"),
        P("fs", "tp"),
        P("tp", "fs"),
        P(("fs", "tp"), None),
    )
    out_specs = (P(("fs", "tp"), None), P("fs", "tp"), P("fs", "tp"), P("tp", "fs"))
    return jax.shard_map(body, mesh=mesh, in_specs=in_specs, out_specs=out_specs, check_vma=False)
```

profile of v0, /device:TPU:0, one launch (start us, length us, event | category | flops | bytes accessed | tf_op | source)
XLA Modules:
  0.0 514.1 jit_solution(16898894607041836768)
XLA Ops:
  7.2 0.0 all-gather.12.cloned.1.call-start
  7.2 0.7 all-gather.12.cloned.1.call-update
  7.9 0.0 all-gather.10.cloned.1.call-start
  7.9 0.7 all-gather.10.cloned.1.call-update
  8.6 0.0 all-gather.14.cloned.1.call-start
  8.7 0.7 all-gather.14.cloned.1.call-update
  9.4 0.0 all-gather.8.cloned.1.call-start
  9.4 0.5 all-gather.8.cloned.1.call-update
  10.0 0.0 all-gather.6.cloned.1.call-start
  10.0 0.5 all-gather.6.cloned.1.call-update
  10.5 0.0 reduce-scatter.3.cloned.1.call-start
  10.6 43.5 %all-gather.12.cloned.1.call-done = bf16[2048,704]{0,1:T(8,128)(2,1)} async-done(((bf16[512,704]{0,1:T(8,128)(2,1)}), bf16[2048,704]{0,1:T(8,128)(2,1)}) %all-gather.12.cloned.1.call-update) | async-done | bytes 2883600 | tf_op jit(solution)/shard_map/all_gather | solution.py:26
  54.1 48.5 %all-gather.10.cloned.1.call-done = bf16[1024,2048]{1,0:T(8,128)(2,1)} async-done(((bf16[128,2048]{1,0:T(8,128)(2,1)}), bf16[1024,2048]{1,0:T(8,128)(2,1)}) %all-gather.10.cloned.1.call-update) | async-done | bytes 4194320 | tf_op jit(solution)/shard_map/all_gather | solution.py:21
  102.6 7.8 %fusion.3 = f32[1024,704]{0,1:T(8,128)} fusion(bf16[1024,2048]{1,0:T(8,128)(2,1)} %all-gather.10.cloned.1.call-done, bf16[2048,704]{0,1:T(8,128)(2,1)} %all-gather.12.cloned.1.call-done), kind=kOutput, calls=%fused_computation.12 | convolution fusion | flops 2952790016 | bytes 9961472 | tf_op jit(solution)/shard_map/dot_general | solution.py:30
  110.4 34.4 %all-gather.14.cloned.1.call-done = bf16[2048,704]{0,1:T(8,128)(2,1)} async-done(((bf16[512,704]{0,1:T(8,128)(2,1)}), bf16[2048,704]{0,1:T(8,128)(2,1)}) %all-gather.14.cloned.1.call-update) | async-done | bytes 2883600 | tf_op jit(solution)/shard_map/all_gather | solution.py:25
  144.8 7.9 %fusion.4 = f32[1024,704]{0,1:T(8,128)} fusion(bf16[1024,2048]{1,0:T(8,128)(2,1)} %all-gather.10.cloned.1.call-done, bf16[2048,704]{0,1:T(8,128)(2,1)} %all-gather.14.cloned.1.call-done), kind=kOutput, calls=%fused_computation.13 | convolution fusion | flops 2952790016 | bytes 9961472 | tf_op jit(solution)/shard_map/dot_general | solution.py:29
  152.7 35.3 %all-gather.8.cloned.1.call-done = bf16[704,2048]{1,0:T(8,128)(2,1)} async-done(((bf16[704,512]{1,0:T(8,128)(2,1)}), bf16[704,2048]{1,0:T(8,128)(2,1)}) %all-gather.8.cloned.1.call-update) | async-done | bytes 2883600 | tf_op jit(solution)/shard_map/all_gather | solution.py:28
  188.1 48.3 %all-gather.6.cloned.1.call-done = bf16[1024,2048]{1,0:T(8,128)(2,1)} async-done(((bf16[128,2048]{1,0:T(8,128)(2,1)}), bf16[1024,2048]{1,0:T(8,128)(2,1)}) %all-gather.6.cloned.1.call-update) | async-done | bytes 4194320 | tf_op jit(solution)/shard_map/all_gather | solution.py:22
  236.4 8.6 %multiply_convert_fusion.1 = (bf16[1024,704]{0,1:T(8,128)(2,1)S(1)}, bf16[1024,704]{0,1:T(8,128)(2,1)S(1)}) fusion(f32[1024,704]{0,1:T(8,128)} %fusion.4, f32[1024,704]{0,1:T(8,128)} %fusion.3, bf16[1024,2048]{1,0:T(8,128)(2,1)} %all-gather.6.cloned.1.call-done, bf16[704,2048]{1,0:T(8,128)(2,1)} %all-gather.8.cloned.1.call-done), kind=kOutput, calls=%fused_computation.6 | convolution fusion | flops 2962161664 | bytes 15728640 | tf_op jit(solution)/shard_map/dot_general | solution.py:14
  245.1 3.5 fusion.5
  248.6 6.1 %convolution_add_fusion = f32[1024,2048]{1,0:T(8,128)} fusion(f32[1024,2048]{1,0:T(8,128)S(1)} %fusion.5, bf16[1024,704]{0,1:T(8,128)(2,1)S(1)} %get-tuple-element.4, bf16[2048,704]{0,1:T(8,128)(2,1)S(1)} %copy-done.2), kind=kOutput, calls=%fused_computation.1 | convolution fusion | flops 2954887168 | bytes 21102592 | tf_op jit(solution)/shard_map/dot_general | solution.py:14
  254.8 0.0 reduce-scatter.5.cloned.1.call-start
  254.8 1.3 copy-done.5
  256.1 5.1 convolution_bitcast_fusion.1
  261.2 3.2 convolution_bitcast_fusion.2
  264.4 0.7 copy-done.9
  265.1 3.2 convolution_bitcast_fusion
  268.3 6.5 %pad_maximum_fusion = f32[2048,2112]{0,1:T(8,128)} fusion(f32[2048,704]{0,1:T(8,128)S(1)} %convolution_bitcast_fusion, f32[2048,704]{0,1:T(8,128)S(1)} %convolution_bitcast_fusion.1, f32[2048,704]{0,1:T(8,128)S(1)} %convolution_bitcast_fusion.2), kind=kLoop, calls=%fused_computation | loop fusion | flops 8650752 | bytes 34603008 | tf_op jit(solution)/shard_map/concatenate | solution.py:47
  274.9 68.4 %reduce-scatter.3.cloned.1.call-done = f32[128,2048]{1,0:T(8,128)} async-done(((f32[1024,2048]{1,0:T(8,128)}), f32[128,2048]{1,0:T(8,128)}) %reduce-scatter.3.cloned.1.call-update) | async-done | bytes 1048592 | tf_op jit(solution)/shard_map/reduce_scatter | solution.py:39
  343.2 2.1 convert_element_type.14
  345.3 157.5 %reduce-scatter.5.cloned.1.call-done = f32[512,2112]{0,1:T(8,128)} async-done(((f32[2048,2112]{0,1:T(8,128)}), f32[512,2112]{0,1:T(8,128)}) %reduce-scatter.5.cloned.1.call-update) | async-done | bytes 4325392 | tf_op jit(solution)/shard_map/reduce_scatter | solution.py:46
  502.8 4.4 slice_bitcast_fusion
  (20 shorter events, 0.1 us)
Async XLA Ops:
  7.2 46.9 %all-gather.12.cloned.1.call-start = ((), (), s32[]{:S(2)}) async-start(), calls=%async_computation.5 | async-start | bytes 3604480 | tf_op jit(solution)/shard_map/all_gather | solution.py:26
  7.9 94.7 %all-gather.10.cloned.1.call-start = ((), (), s32[]{:S(2)}) async-start(), calls=%async_computation.4 | async-start | bytes 4718592 | tf_op jit(solution)/shard_map/all_gather | solution.py:21
  8.6 136.2 %all-gather.14.cloned.1.call-start = ((), (), s32[]{:S(2)}) async-start(), calls=%async_computation.6 | async-start | bytes 3604480 | tf_op jit(solution)/shard_map/all_gather | solution.py:25
  9.4 178.7 %all-gather.8.cloned.1.call-start = ((), (), s32[]{:S(2)}) async-start(), calls=%async_computation.3 | async-start | bytes 3604480 | tf_op jit(solution)/shard_map/all_gather | solution.py:28
  10.0 226.4 %all-gather.6.cloned.1.call-start = ((), (), s32[]{:S(2)}) async-start(), calls=%async_computation.2 | async-start | bytes 4718592 | tf_op jit(solution)/shard_map/all_gather | solution.py:22
  10.5 332.7 %reduce-scatter.3.cloned.1.call-start = ((), (), s32[]{:S(2)}) async-start(), calls=%async_computation.7 | async-start | bytes 9437184 | tf_op jit(solution)/shard_map/reduce_scatter | solution.py:39
  152.7 92.3 %copy-start.3 = (bf16[2048,704]{0,1:T(8,128)(2,1)S(1)}, bf16[2048,704]{0,1:T(8,128)(2,1)}, u32[]{:S(2)}) copy-start(bf16[2048,704]{0,1:T(8,128)(2,1)} %all-gather.14.cloned.1.call-done) | copy-start | bytes 8650756
  245.0 3.6 copy-start.6
  245.0 3.6 copy-start.4
  245.1 3.6 copy-start.2
  254.7 1.4 copy-start.5
  254.7 6.4 %copy-start.7 = (bf16[1024,704]{0,1:T(8,128)(2,1)S(1)}, bf16[1024,704]{0,1:T(8,128)(2,1)}, u32[]{:S(2)}) copy-start(bf16[1024,704]{0,1:T(8,128)(2,1)} %copy-done.6) | copy-start | bytes 4325380
  254.8 248.1 %reduce-scatter.5.cloned.1.call-start = ((), (), s32[]{:S(2)}) async-start(), calls=%async_computation.8 | async-start | bytes 21626880 | tf_op jit(solution)/shard_map/reduce_scatter | solution.py:46
  256.1 5.1 copy-start
  261.2 3.2 copy-start.1
  261.2 3.2 copy-start.8
  261.2 3.9 copy-start.9
Sparse Core Ops, SparseCore 0:
  9.8 44.2 all-gather.11
  55.7 46.8 all-gather.9
  104.4 40.3 all-gather.13
  146.5 41.5 all-gather.7
  189.5 46.8 all-gather.5
  254.9 88.3 reduce-scatter.2
  346.4 156.4 reduce-scatter.4
where the time goes:
time: 514 us
  waiting for transfers between devices  439 us (85%)
  matrix products  45.4 us (9%)
  between operations  14.3 us (3%)
  other arithmetic  8.6 us (2%)
  local copies, waits for them, and re-layouts  6.37 us (1%)
    reduce_scatter x1, waiting for transfers between devices, body(): lax.psum_scatter(jnp.concatenate([over_rows(tok_all, d_gate), over_rows(t...  158 us
    reduce_scatter x1, waiting for transfers between devices, body(): lax.psum_scatter(over_cols(d_gate, gate_full) + over_cols(d_up, up_full),...  68.4 us
    all_gather x1, waiting for transfers between devices, body(): lax.all_gather(tokens, 'tp', axis=0, tiled=True)  48.5 us
    all_gather x1, waiting for transfers between devices, body(): lax.all_gather(grad_out, 'tp', axis=0, tiled=True)  48.3 us
    all_gather x1, waiting for transfers between devices, body(): lax.all_gather(up_weight, 'fs', axis=0, tiled=True)  43.5 us
    all_gather x1, waiting for transfers between devices, body(): down_full = lax.all_gather(down_weight, 'fs', axis=1, tiled=True)  35.3 us
    all_gather x1, waiting for transfers between devices, body(): lax.all_gather(gate_weight, 'fs', axis=0, tiled=True)  34.4 us
    dot_general x3, matrix products, over_cols(): lax.dot_general(left, right, (((1,), (1,)), ((), ())), preferred_element_...  18.2 us
  transfers between devices with their start and end apart: 7, of which 7 were waited for; matrix products, arithmetic and copies ran while one was open for 7% of the time, Pallas kernels for 0%

commit v1 on v0

--- a/solution.py
+++ b/solution.py
@@ -25,7 +25,12 @@
         lax.all_gather(gate_weight, "fs", axis=0, tiled=True),
         lax.all_gather(up_weight, "fs", axis=0, tiled=True),
     )
-    down_full = lax.all_gather(down_weight, "fs", axis=1, tiled=True)
+    ring = [down_weight]
+    for hop in range(3):
+        ring.append(lax.ppermute(ring[-1], "fs", [(dev, (dev + 1) % 4) for dev in range(4)]))
+    down_full = jnp.roll(
+        jnp.concatenate(ring[::-1], axis=1), (lax.axis_index("fs") + 1) * ring[0].shape[1], axis=1
+    )
     gate_pre = jnp.dot(tok_all, gate_full, preferred_element_type=jnp.float32)
     up_pre = jnp.dot(tok_all, up_full, preferred_element_type=jnp.float32)
     sig_gate = jax.nn.sigmoid(gate_pre)

time: 514 us -> 491 us (0.955)
  waiting for transfers between devices: 439 us -> 402 us
  local copies, waits for them, and re-layouts: 6.37 us -> 14.4 us
  starting transfers between devices: 0.27 us -> 6.22 us
    ppermute x0 -> x3, waiting for transfers between devices: none -> 69.2 us  [body(): lax.ppermute(ring[-1], 'fs', [(dev, (dev + 1) % 4) for dev in range(4)])]
    all_gather x1 -> x0, waiting for transfers between devices: 35.3 us -> none  [body(): down_full = lax.all_gather(down_weight, 'fs', axis=1, tiled=True)]
    all_gather x1, waiting for transfers between devices: 34.4 us -> 0.01 us  [body(): lax.all_gather(gate_weight, 'fs', axis=0, tiled=True)]
    all_gather x1, waiting for transfers between devices: 48.5 us -> 29.6 us  [body(): lax.all_gather(tokens, 'tp', axis=0, tiled=True)]
    all_gather x1, waiting for transfers between devices: 43.5 us -> 34.4 us  [body(): lax.all_gather(up_weight, 'fs', axis=0, tiled=True)]
    all_gather x1, waiting for transfers between devices: 48.3 us -> 40.5 us  [body(): lax.all_gather(grad_out, 'tp', axis=0, tiled=True)]
    unnamed x20 -> x29, local copies, waits for them, and re-layouts: 1.99 us -> 8.97 us
    ppermute x0 -> x3, starting transfers between devices: none -> 5.99 us  [body(): lax.ppermute(ring[-1], 'fs', [(dev, (dev + 1) % 4) for dev in range(4)])]
  transfers between devices with their start and end apart: 7 -> 9, of which waited for: 7 -> 8; matrix products, arithmetic and copies ran while one was open for 7% -> 9% of each run, Pallas kernels for 0% -> 0%
where the time goes in v1:
time: 491 us
  waiting for transfers between devices  402 us (82%)
  matrix products  45.5 us (9%)
  local copies, waits for them, and re-layouts  14.4 us (3%)
  between operations  14.3 us (3%)
  other arithmetic  8.63 us (2%)
  starting transfers between devices  6.22 us (1%)
    reduce_scatter x1, waiting for transfers between devices, body(): lax.psum_scatter(jnp.concatenate([over_rows(tok_all, d_gate), over_rows(t...  157 us
    ppermute x3, waiting for transfers between devices, body(): lax.ppermute(ring[-1], 'fs', [(dev, (dev + 1) % 4) for dev in range(4)])  69.2 us
    reduce_scatter x1, waiting for transfers between devices, body(): lax.psum_scatter(over_cols(d_gate, gate_full) + over_cols(d_up, up_full),...  68.3 us
    all_gather x1, waiting for transfers between devices, body(): lax.all_gather(grad_out, 'tp', axis=0, tiled=True)  40.5 us
    all_gather x1, waiting for transfers between devices, body(): lax.all_gather(up_weight, 'fs', axis=0, tiled=True)  34.4 us
    all_gather x1, waiting for transfers between devices, body(): lax.all_gather(tokens, 'tp', axis=0, tiled=True)  29.6 us
    dot_general x3, matrix products, over_cols(): lax.dot_general(left, right, (((1,), (1,)), ((), ())), preferred_element_...  18.3 us
    dot_general x3, matrix products, over_rows(): lax.dot_general(left, right, (((0,), (0,)), ((), ())), preferred_element_...  11.5 us
  transfers between devices with their start and end apart: 9, of which 8 were waited for; matrix products, arithmetic and copies ran while one was open for 9% of the time, Pallas kernels for 0%

profile of v1, /device:TPU:0, one launch (start us, length us, event | category | flops | bytes accessed | tf_op | source)
XLA Modules:
  0.0 490.9 jit_solution(16946775046541042557)
XLA Ops:
  7.9 0.7 all-gather.7.cloned.1.call-update
  10.0 3.0 collective-permute-start
  13.0 24.7 %collective-permute-done = bf16[704,512]{1,0:T(8,128)(2,1)S(1)} collective-permute-done((bf16[704,512]{1,0:T(8,128)(2,1)}, bf16[704,512]{1,0:T(8,128)(2,1)S(1)}, u32[]{:S(2)}, u32[]{:S(2)}) %collective-permute-start) | collective-permute-done | bytes 720928 | tf_op jit(solution)/shard_map/ppermute | solution.py:30
  37.8 1.1 collective-permute-start.1
  38.8 28.5 %collective-permute-done.1 = bf16[704,512]{1,0:T(8,128)(2,1)S(1)} collective-permute-done((bf16[704,512]{1,0:T(8,128)(2,1)S(1)}, bf16[704,512]{1,0:T(8,128)(2,1)S(1)}, u32[]{:S(2)}, u32[]{:S(2)}) %collective-permute-start.1) | collective-permute-done | bytes 720928 | tf_op jit(solution)/shard_map/ppermute | solution.py:30
  67.4 1.9 collective-permute-start.2
  69.3 15.9 %collective-permute-done.2 = bf16[704,512]{1,0:T(8,128)(2,1)S(1)} collective-permute-done((bf16[704,512]{1,0:T(8,128)(2,1)S(1)}, bf16[704,512]{1,0:T(8,128)(2,1)S(1)}, u32[]{:S(2)}, u32[]{:S(2)}) %collective-permute-start.2) | collective-permute-done | bytes 720928 | tf_op jit(solution)/shard_map/ppermute | solution.py:30
  85.2 1.0 constant_dynamic-update-slice_fusion.7
  86.2 1.1 constant_dynamic-update-slice_fusion.6
  87.3 0.9 constant_dynamic-update-slice_fusion.5
  88.2 1.0 constant_dynamic-update-slice_fusion.4
  89.2 1.0 constant_dynamic-update-slice_fusion.3
  90.2 1.0 constant_dynamic-update-slice_fusion.2
  91.2 1.0 constant_dynamic-update-slice_fusion.1
  92.1 1.0 constant_dynamic-update-slice_fusion
  93.2 29.6 %all-gather.7.cloned.1.call-done = bf16[1024,2048]{1,0:T(8,128)(2,1)} async-done(((bf16[128,2048]{1,0:T(8,128)(2,1)}), bf16[1024,2048]{1,0:T(8,128)(2,1)}) %all-gather.7.cloned.1.call-update) | async-done | bytes 4194320 | tf_op jit(solution)/shard_map/all_gather | solution.py:21
  122.7 7.8 %fusion.11 = f32[1024,704]{0,1:T(8,128)} fusion(bf16[1024,2048]{1,0:T(8,128)(2,1)} %all-gather.7.cloned.1.call-done, bf16[2048,704]{0,1:T(8,128)(2,1)} %all-gather.11.cloned.1.call-done), kind=kOutput, calls=%fused_computation.28 | convolution fusion | flops 2952790016 | bytes 9961472 | tf_op jit(solution)/shard_map/dot_general | solution.py:34
  130.5 34.4 %all-gather.9.cloned.1.call-done = bf16[2048,704]{0,1:T(8,128)(2,1)} async-done(((bf16[512,704]{0,1:T(8,128)(2,1)}), bf16[2048,704]{0,1:T(8,128)(2,1)}) %all-gather.9.cloned.1.call-update) | async-done | bytes 2883600 | tf_op jit(solution)/shard_map/all_gather | solution.py:26
  164.9 7.9 %fusion.10 = f32[1024,704]{0,1:T(8,128)} fusion(bf16[1024,2048]{1,0:T(8,128)(2,1)} %all-gather.7.cloned.1.call-done, bf16[2048,704]{0,1:T(8,128)(2,1)} %all-gather.9.cloned.1.call-done), kind=kOutput, calls=%fused_computation.27 | convolution fusion | flops 2952790016 | bytes 9961472 | tf_op jit(solution)/shard_map/dot_general | solution.py:35
  172.8 40.5 %all-gather.5.cloned.1.call-done = bf16[1024,2048]{1,0:T(8,128)(2,1)} async-done(((bf16[128,2048]{1,0:T(8,128)(2,1)}), bf16[1024,2048]{1,0:T(8,128)(2,1)}) %all-gather.5.cloned.1.call-update) | async-done | bytes 4194320 | tf_op jit(solution)/shard_map/all_gather | solution.py:22
  213.3 8.7 %fusion.3 = (bf16[1024,704]{0,1:T(8,128)(2,1)S(1)}, bf16[1024,704]{0,1:T(8,128)(2,1)S(1)}) fusion(f32[1024,704]{0,1:T(8,128)} %fusion.11, f32[1024,704]{0,1:T(8,128)} %fusion.10, bf16[1024,2048]{1,0:T(8,128)(2,1)} %all-gather.5.cloned.1.call-done, bf16[704,4096]{1,0:T(8,128)(2,1)} %constant_dynamic-update-slice_fusion, s32[]{:T(128)S(6)} %select_n.14), kind=kOutput, calls=%fused_computation.10 | convolution fusion | flops 2962161664 | bytes 15728644 | tf_op jit(solution)/shard_map/dot_general | solution.py:14
  222.0 3.7 fusion.12
  225.7 6.0 %convolution_add_fusion = f32[1024,2048]{1,0:T(8,128)} fusion(f32[1024,2048]{1,0:T(8,128)S(1)} %fusion.12, bf16[1024,704]{0,1:T(8,128)(2,1)S(1)} %get-tuple-element.4, bf16[2048,704]{0,1:T(8,128)(2,1)S(1)} %copy-done.4), kind=kOutput, calls=%fused_computation.1 | convolution fusion | flops 2954887168 | bytes 21102592 | tf_op jit(solution)/shard_map/dot_general | solution.py:14
  231.8 1.3 copy-done.6
  233.1 5.1 %convolution_bitcast_fusion.1 = f32[2048,704]{0,1:T(8,128)S(1)} fusion(bf16[1024,704]{0,1:T(8,128)(2,1)S(1)} %copy-done.6, bf16[1024,2048]{1,0:T(8,128)(2,1)} %all-gather.7.cloned.1.call-done), kind=kOutput, calls=%fused_computation.3 | convolution fusion | flops 2952790016 | bytes 11403264 | tf_op jit(solution)/shard_map/dot_general | solution.py:8
  238.2 3.2 convolution_bitcast_fusion.2
  242.1 3.2 convolution_bitcast_fusion
  245.3 6.5 %pad_maximum_fusion = f32[2048,2112]{0,1:T(8,128)} fusion(f32[2048,704]{0,1:T(8,128)S(1)} %convolution_bitcast_fusion, f32[2048,704]{0,1:T(8,128)S(1)} %convolution_bitcast_fusion.1, f32[2048,704]{0,1:T(8,128)S(1)} %convolution_bitcast_fusion.2), kind=kLoop, calls=%fused_computation | loop fusion | flops 8650752 | bytes 34603008 | tf_op jit(solution)/shard_map/concatenate | solution.py:52
  251.9 68.3 %reduce-scatter.3.cloned.1.call-done = f32[128,2048]{1,0:T(8,128)} async-done(((f32[1024,2048]{1,0:T(8,128)}), f32[128,2048]{1,0:T(8,128)}) %reduce-scatter.3.cloned.1.call-update) | async-done | bytes 1048592 | tf_op jit(solution)/shard_map/reduce_scatter | solution.py:44
  320.2 2.1 convert_element_type.14
  322.3 157.4 %reduce-scatter.5.cloned.1.call-done = f32[512,2112]{0,1:T(8,128)} async-done(((f32[2048,2112]{0,1:T(8,128)}), f32[512,2112]{0,1:T(8,128)}) %reduce-scatter.5.cloned.1.call-update) | async-done | bytes 4325392 | tf_op jit(solution)/shard_map/reduce_scatter | solution.py:51
  479.7 4.4 slice_bitcast_fusion
  (33 shorter events, 2.9 us)
Async XLA Ops:
  7.2 86.0 %all-gather.11.cloned.1.call-start = ((), (), s32[]{:S(2)}) async-start(), calls=%async_computation.5 | async-start | bytes 3604480 | tf_op jit(solution)/shard_map/all_gather | solution.py:25
  7.9 114.8 %all-gather.7.cloned.1.call-start = ((), (), s32[]{:S(2)}) async-start(), calls=%async_computation.3 | async-start | bytes 4718592 | tf_op jit(solution)/shard_map/all_gather | solution.py:21
  8.6 79.6 %copy-start = (bf16[704,512]{1,0:T(8,128)(2,1)S(1)}, bf16[704,512]{1,0:T(8,128)(2,1)}, u32[]{:S(2)}) copy-start(bf16[704,512]{1,0:T(8,128)(2,1)} %param.8) | copy-start | bytes 2162692
  8.7 156.3 %all-gather.9.cloned.1.call-start = ((), (), s32[]{:S(2)}) async-start(), calls=%async_computation.4 | async-start | bytes 3604480 | tf_op jit(solution)/shard_map/all_gather | solution.py:26
  9.4 203.9 %all-gather.5.cloned.1.call-start = ((), (), s32[]{:S(2)}) async-start(), calls=%async_computation.2 | async-start | bytes 4718592 | tf_op jit(solution)/shard_map/all_gather | solution.py:22
  10.0 310.3 %reduce-scatter.3.cloned.1.call-start = ((), (), s32[]{:S(2)}) async-start(), calls=%async_computation.6 | async-start | bytes 9437184 | tf_op jit(solution)/shard_map/reduce_scatter | solution.py:44
  10.0 27.8 %collective-permute-start = (bf16[704,512]{1,0:T(8,128)(2,1)}, bf16[704,512]{1,0:T(8,128)(2,1)S(1)}, u32[]{:S(2)}, u32[]{:S(2)}) collective-permute-start(bf16[704,512]{1,0:T(8,128)(2,1)} %param.8), channel_id=1, source_target_pairs={{0,8},{8,16},{16,24},{24,0},{1,9},{9,17},{17,25},{25,1},{2,10},{10... | collective-permute-start | bytes 2162696 | tf_op jit(solution)/shard_map/ppermute | solution.py:30
  37.8 29.6 %collective-permute-start.1 = (bf16[704,512]{1,0:T(8,128)(2,1)S(1)}, bf16[704,512]{1,0:T(8,128)(2,1)S(1)}, u32[]{:S(2)}, u32[]{:S(2)}) collective-permute-start(bf16[704,512]{1,0:T(8,128)(2,1)S(1)} %collective-permute-done), channel_id=1, source_target_pairs={{0,8},{8,16},{16,24},{24,0},{1,9},{9,17},{17,25},{25,1},{2,10},{10... | collective-permute-start | bytes 2162696 | tf_op jit(solution)/shard_map/ppermute | solution.py:30
  67.4 17.8 %collective-permute-start.2 = (bf16[704,512]{1,0:T(8,128)(2,1)S(1)}, bf16[704,512]{1,0:T(8,128)(2,1)S(1)}, u32[]{:S(2)}, u32[]{:S(2)}) collective-permute-start(bf16[704,512]{1,0:T(8,128)(2,1)S(1)} %collective-permute-done.1), channel_id=1, source_target_pairs={{0,8},{8,16},{16,24},{24,0},{1,9},{9,17},{17,25},{25,1},{2,10},{10... | collective-permute-start | bytes 2162696 | tf_op jit(solution)/shard_map/ppermute | solution.py:30
  172.8 49.2 %copy-start.3 = (bf16[2048,704]{0,1:T(8,128)(2,1)S(1)}, bf16[2048,704]{0,1:T(8,128)(2,1)}, u32[]{:S(2)}) copy-start(bf16[2048,704]{0,1:T(8,128)(2,1)} %all-gather.11.cloned.1.call-done) | copy-start | bytes 8650756
  222.0 3.8 copy-start.7
  222.0 3.8 copy-start.5
  222.0 3.7 copy-start.4
  231.7 1.4 copy-start.6
  231.7 6.4 %copy-start.8 = (bf16[1024,704]{0,1:T(8,128)(2,1)S(1)}, bf16[1024,704]{0,1:T(8,128)(2,1)}, u32[]{:S(2)}) copy-start(bf16[1024,704]{0,1:T(8,128)(2,1)} %copy-done.7) | copy-start | bytes 4325380
  231.8 247.9 %reduce-scatter.5.cloned.1.call-start = ((), (), s32[]{:S(2)}) async-start(), calls=%async_computation.7 | async-start | bytes 21626880 | tf_op jit(solution)/shard_map/reduce_scatter | solution.py:51
  233.1 5.1 %copy-start.1 = (bf16[1024,2048]{1,0:T(8,128)(2,1)S(1)}, bf16[1024,2048]{1,0:T(8,128)(2,1)}, u32[]{:S(2)}) copy-start(bf16[1024,2048]{1,0:T(8,128)(2,1)} %all-gather.7.cloned.1.call-done) | copy-start | bytes 12582916
  238.2 3.2 copy-start.2
  238.2 3.2 copy-start.9
  238.2 3.9 copy-start.10
Sparse Core Ops, SparseCore 0:
  9.8 64.7 all-gather.10
  76.1 46.5 all-gather.6
  124.6 40.3 all-gather.8
  166.4 46.8 all-gather.4
  231.9 88.3 reduce-scatter.2
  323.2 156.4 reduce-scatter.4
